TPU v7x, 32 devices: a whole 2x2x4 slice. The times are simulated.
32 devices in a mesh: gr: 2 (over x), sp: 8 (over z, y), tp: 2 (over core).
Axes of the slice: x: 2, y: 2, z: 4, core: 2. Of those that a mesh axis runs over, the one named last changes fastest.
Arguments:
- tokens: bfloat16 [8, 1536, 4096], P('gr', 'sp', 'tp'), may hold values from -6.5 to 6.5
- first_token_input: bfloat16 [8, 4096], P('gr', 'sp'), may hold values from -6 to 6
- forget_weight: bfloat16 [4096, 4096], P(None, 'tp'), may hold values from -0.1171875 to 0.1171875
- value_weight: bfloat16 [4096, 4096], P(None, 'tp'), may hold values from -0.375 to 0.375
- query_weight: bfloat16 [4096, 4096], P('sp', 'tp'), may hold values from -0.09375 to 0.09375
- output_gate_weight: bfloat16 [4096, 4096], P('sp', 'tp'), may hold values from -0.09375 to 0.09375
- forget_bound_slack: float32 [4096], P('tp'), may hold values from 0.00032552083 to 0.8, as said below
- additional_damping_exponent: float32 [8, 1536, 32], P('gr', 'sp', 'tp'), may hold values from -2.2 to 0, as said below
- read_norm_scale: float32 [128], replicated, may hold values from 0.1 to 1.9
Outputs:
- cache: bfloat16 [8, 32, 128, 128], P('gr', 'tp', 'sp')
- first_read: bfloat16 [8, 4096], P('gr', 'tp')
Inputs may be any that keep to these rules, and one draw needn't show every extreme that they name: `forget_bound_slack`: positive gaps, one per channel. `additional_damping_exponent`: non-positive log-decays.
All inputs are finite; a program needn't handle non-finite values.
Results may differ from a plain program's by a relative error of at most 0.018.
Values may be sent and summed in bfloat16 or wider, within the bound.
A program may use at most 128 MiB of HBM per device.

v0:
```python
import jax
import jax.numpy as jnp
from jax import lax
from jax.sharding import PartitionSpec as P


def carried_in(value, axis, join, neutral):
    count, mine = (lax.axis_size(axis), lax.axis_index(axis))
    pieces = lax.all_gather(value, axis)
    pieces = pieces[::-1]
    mine = count - 1 - mine
    total = jnp.full_like(value, 0) + jnp.asarray(neutral, value.dtype)

    def turn(position, total):
        longer = join(total, pieces[position])
        return jnp.where(position < mine, longer, total)

    return lax.fori_loop(0, count - 1, turn, total)


def add_sums(earlier, later_part):
    return earlier + later_part


def per_device(
    tokens,
    first_token_input,
    forget_weight,
    value_weight,
    query_weight,
    output_gate_weight,
    forget_bound_slack,
    additional_damping_exponent,
    read_norm_scale,
):
    seq_count, block_len, width_part = tokens.shape
    head_dim = read_norm_scale.shape[0]
    local_heads = additional_damping_exponent.shape[2]
    channels = local_heads * head_dim
    flat_rows = tokens.reshape(seq_count * block_len, width_part)
    segment = lax.all_gather(flat_rows, "tp", axis=1, tiled=True)
    forget_acc = jnp.dot(segment, forget_weight, preferred_element_type=jnp.float32)
    value_acc = jnp.dot(segment, value_weight, preferred_element_type=jnp.float32)
    forget = forget_acc.astype(jnp.bfloat16).reshape(seq_count, block_len, channels)
    values = value_acc.astype(jnp.bfloat16).reshape(seq_count, block_len, local_heads, head_dim)
    sp_count = lax.axis_size("sp")
    rows_here = head_dim // sp_count
    row_start = lax.axis_index("sp") * rows_here
    valve_sampler_seeds = forget_bound_slack * jax.nn.sigmoid(-forget.astype(jnp.float32))
    damping_exponent = jnp.log1p(-valve_sampler_seeds) + jnp.repeat(
        additional_damping_exponent, head_dim, axis=2
    )
    totals = jnp.sum(damping_exponent, axis=1)
    later_sum = carried_in(totals, "sp", add_sums, jnp.zeros_like(totals))
    within = totals[:, None, :] - jnp.cumsum(damping_exponent, axis=1)
    weighted = (valve_sampler_seeds * jnp.exp(within + later_sum[:, None, :])).astype(jnp.bfloat16)
    weighted = weighted.reshape(seq_count, block_len, local_heads, head_dim)
    state_terms = jnp.einsum(
        "slha,slhb->shab", weighted, values, preferred_element_type=jnp.float32
    )
    state_sum = lax.psum_scatter(state_terms, "sp", scatter_dimension=2, tiled=True)
    cache_rows = state_sum.astype(jnp.bfloat16)
    slab_rows = first_token_input.shape[1]
    row_first = lax.axis_index("sp") * slab_rows
    forget_rows = lax.dynamic_slice_in_dim(forget_weight, row_first, slab_rows, 0)
    value_rows = lax.dynamic_slice_in_dim(value_weight, row_first, slab_rows, 0)
    new_sums = lax.psum(
        (
            jnp.dot(first_token_input, query_weight, preferred_element_type=jnp.float32),
            jnp.dot(first_token_input, output_gate_weight, preferred_element_type=jnp.float32),
            jnp.dot(first_token_input, forget_rows, preferred_element_type=jnp.float32),
            jnp.dot(first_token_input, value_rows, preferred_element_type=jnp.float32),
        ),
        "sp",
    )
    new_query, new_gate, new_forget, new_value = [
        summed.astype(jnp.bfloat16) for summed in new_sums
    ]
    new_keys = (forget_bound_slack * jax.nn.sigmoid(-new_forget.astype(jnp.float32))).reshape(
        seq_count, local_heads, head_dim
    )
    own_keys = lax.dynamic_slice_in_dim(new_keys, row_start, rows_here, 2)
    own_query = lax.dynamic_slice_in_dim(
        new_query.astype(jnp.float32).reshape(seq_count, local_heads, head_dim),
        row_start,
        rows_here,
        2,
    )
    value_new = new_value.astype(jnp.float32).reshape(seq_count, local_heads, head_dim)
    updated = (1.0 - own_keys)[..., None] * cache_rows.astype(jnp.float32) + own_keys[
        ..., None
    ] * value_new[:, :, None, :]
    read_part = jnp.einsum("sha,shab->shb", own_query, updated, precision=lax.Precision.HIGHEST)
    read_sum = lax.psum(read_part, "sp")
    scaled = (
        read_sum
        * lax.rsqrt(jnp.mean(read_sum * read_sum, axis=-1, keepdims=True) + 1e-06)
        * read_norm_scale
    )
    first_read = (
        scaled.reshape(seq_count, channels) * jax.nn.silu(new_gate.astype(jnp.float32))
    ).astype(jnp.bfloat16)
    return (cache_rows, first_read)


def solution(mesh):
    placed = (
        P("gr", "sp", "tp"),
        P("gr", "sp"),
        P(None, "tp"),
        P(None, "tp"),
        P("sp", "tp"),
        P("sp", "tp"),
        P("tp"),
        P("gr", "sp", "tp"),
        P(),
    )
    return jax.shard_map(
        per_device,
        mesh=mesh,
        in_specs=placed,
        out_specs=(P("gr", "tp", "sp", None), P("gr", "tp")),
        check_vma=False,
    )
```

profile of v0, /device:TPU:0, one launch (start us, length us, event | category | flops | bytes accessed | tf_op | source)
XLA Modules:
  0.0 277.1 jit_solution(17281047717059468715)
XLA Ops:
  7.2 0.0 copy-start
  7.2 0.0 all-gather.2.cloned.1.call-start
  7.2 0.7 all-gather.2.cloned.1.call-update
  7.9 0.0 reduce-scatter.2.cloned.1.call-start
  8.0 1.0 copy.18
  9.0 3.8 %broadcast_in_dim.4 = f32[4,192,16,128]{3,2,1,0:T(8,128)} broadcast(f32[4,192,16]{2,1,0:T(8,128)S(1)} %copy.18), dimensions={0,1,2} | broadcast | bytes 6340608 | tf_op jit(solution)/shard_map/broadcast_in_dim | solution.py:50
  12.8 7.3 %reshape.70 = f32[4,192,2048]{2,1,0:T(8,128)} reshape(f32[4,192,16,128]{3,2,1,0:T(8,128)} %broadcast_in_dim.4) | data formatting | bytes 12582912 | tf_op jit(solution)/shard_map/reshape | solution.py:50
  20.1 9.0 %all-gather.2.cloned.1.call-done = bf16[768,4096]{1,0:T(8,128)(2,1)} async-done(((bf16[768,2048]{1,0:T(8,128)(2,1)}), bf16[768,4096]{1,0:T(8,128)(2,1)}) %all-gather.2.cloned.1.call-update) | async-done | bytes 6291472 | tf_op jit(solution)/shard_map/all_gather | solution.py:41
  29.0 18.5 %fusion.17 = bf16[96,8,16,128]{3,1,2,0:T(8,128)(2,1)S(1)} fusion(bf16[768,4096]{1,0:T(8,128)(2,1)} %all-gather.2.cloned.1.call-done, bf16[4096,2048]{1,0:T(8,128)(2,1)} %param.14), kind=kOutput, calls=%fused_computation.27 | convolution fusion | flops 12886474752 | bytes 26214400 | tf_op jit(solution)/shard_map/dot_general | solution.py:43
  47.6 0.0 copy-start.8
  47.6 2.6 copy.28
  50.2 1.3 copy-done.8
  51.5 16.8 %add_divide_fusion = f32[768,2048]{1,0:T(8,128)S(1)} fusion(bf16[768,4096]{1,0:T(8,128)(2,1)S(1)} %copy-done.8, bf16[4096,2048]{1,0:T(8,128)(2,1)} %param.13), kind=kOutput, calls=%fused_computation.14 | convolution fusion | flops 12891193344 | bytes 29360128 | tf_op jit(solution)/shard_map/dot_general | solution.py:42
  68.3 0.0 copy-start.5
  68.3 1.5 copy.26
  69.8 1.2 copy-done.1
  71.1 0.0 copy-done.5
  71.1 2.8 %fusion.5 = f32[4,16,128]{2,1,0:T(8,128)S(1)} fusion(f32[4,192,16]{2,1,0:T(8,128)S(1)} %copy.18, f32[16,128]{1,0:T(8,128)S(1)} %bitcast.94, f32[4,192,16,128]{3,2,1,0:T(8,128)S(1)} %bitcast.90), kind=kLoop, calls=%fused_computation.7 | loop fusion | flops 6283264 | bytes 6381568 | tf_op jit(solution)/shard_map/reduce_sum | solution.py:53
  73.9 31.3 %all_gather.11 = f32[8,4,2048]{2,1,0:T(4,128)S(1)} all-gather(f32[1,4,2048]{2,1,0:T(4,128)S(1)} %all_gather.10), channel_id=1, replica_groups=mesh['gr'=2,'sp'=8,'tp'=2] {'sp'}, dimensions={0}, use_global_device_ids=true | all-gather | bytes 294912 | tf_op jit(solution)/shard_map/all_gather | solution.py:9
  105.2 0.3 while.14
  105.6 7.0 %add_bitcast_fusion = f32[4,2048,192]{1,2,0:T(8,128)S(1)} fusion(f32[4,192,2048]{2,1,0:T(8,128)} %reshape.70, f32[4,192,2048]{2,1,0:T(8,128)} %bitcast.86, f32[2048]{0:T(1024)S(1)} %copy-done.5), kind=kLoop, calls=%fused_computation.13 | loop fusion | flops 4718592 | bytes 18882560 | tf_op jit(solution)/shard_map/transpose
  112.6 1.1 pad.3
  113.8 5.6 %fusion = f32[4,2048,2,128]{1,2,3,0:T(2,128)S(1)} fusion(f32[4,2048,2,128]{1,3,2,0:T(8,128)S(1)} %bitcast.88), kind=kOutput, calls=%fused_computation.1 | output fusion | flops 266338304 | bytes 16777216 | tf_op jit(solution)/shard_map/reduce-window
  119.4 3.2 %copy-done.2 = f32[4,2048,2,128]{1,2,3,0:T(2,128)} copy-done((f32[4,2048,2,128]{1,2,3,0:T(2,128)}, f32[4,2048,2,128]{1,2,3,0:T(2,128)S(1)}, u32[]{:S(2)}) %copy-start.2) | copy-done | bytes 8388632
  122.6 0.1 reduce-window.9
  122.8 6.3 %broadcast_add_fusion = f32[4,2048,2,128]{1,2,3,0:T(2,128)S(1)} fusion(f32[4,2048,2,128]{1,2,3,0:T(2,128)} %copy-done.2, f32[4,2048,2]{1,2,0:T(2,128)S(1)} %slice.13), kind=kLoop, calls=%fused_computation.15 | loop fusion | flops 2097152 | bytes 16842752 | tf_op jit(solution)/shard_map/reduce_window_sum
  129.1 4.9 %copy.20 = f32[4,2048,2,128]{1,3,2,0:T(8,128)S(1)} copy(f32[4,2048,2,128]{1,2,3,0:T(2,128)S(1)} %broadcast_add_fusion) | data formatting | bytes 16777216 | tf_op jit(solution)/shard_map/reduce_window_sum
  134.0 0.0 copy-start.6
  134.0 6.2 %fusion.11 = f32[4,16,128,128]{3,2,1,0:T(8,128)} fusion(bf16[4,192,16,128]{3,2,1,0:T(8,128)(2,1)S(1)} %bitcast.91, f32[4,256,2048]{2,1,0:T(8,128)S(1)} %bitcast.89, f32[4,192,2048]{2,1,0:T(8,128)} %bitcast.87, f32[4,2048]{1,0:T(4,128)S(1)} %get-tuple-element.81, f32[4,2048]{1,0:T(4,128)S(1)} %bitcast.95, f32[2048]{0:T(1024)S(1)} %copy-done.5), kind=kOutput, calls=%fused_computation.19 | convolution fusion | flops 410517504 | bytes 19996672 | tf_op jit(solution)/shard_map/slha,slhb->shab/dot_general | solution.py:58
  140.2 0.0 reduce-scatter.2.cloned.1.call-update
  140.2 0.0 copy-start.7
  140.2 0.0 copy-done.6
  140.2 2.0 convolution_bitcast_fusion.1
  142.2 2.0 convolution_bitcast_fusion
  144.2 0.0 copy-done
  144.2 0.4 fusion.33
  144.6 41.0 %all-reduce.2 = (bf16[4,2048]{1,0:T(4,128)(2,1)S(1)}, bf16[4,2048]{1,0:T(4,128)(2,1)S(1)}, bf16[4,2048]{1,0:T(4,128)(2,1)S(1)}) all-reduce(f32[4,2048]{1,0:T(4,128)S(1)} %convolution_bitcast_fusion, f32[4,2048]{1,0:T(4,128)S(1)} %convolution_bitcast_fusion.1, f32[4,2048]{1,0:T(4,128)S(1)} %fusion.33), channel_id=1, replica_groups=mesh['gr'=2,'sp'=8,'tp'=2] {'sp'}, use_global_device_ids=true, to_apply=%region_8.9 | all-reduce | flops 24576 | bytes 147456 | tf_op jit(solution)/shard_map/psum | solution.py:67
  185.7 0.1 dynamic-slice_bitcast_fusion
  185.8 0.1 broadcast_subtract_fusion
  185.9 2.0 fusion.34
  187.9 43.5 %reduce-scatter.2.cloned.1.call-done = f32[4,16,16,128]{3,2,1,0:T(8,128)} async-done(((f32[4,16,128,128]{3,2,1,0:T(8,128)}), f32[4,16,16,128]{3,2,1,0:T(8,128)}) %reduce-scatter.2.cloned.1.call-update) | async-done | bytes 524304 | tf_op jit(solution)/shard_map/reduce_scatter | solution.py:61
  231.4 1.1 convert_element_type.48
  232.5 0.0 copy-start.4
  232.5 0.6 fusion.18
  233.1 36.3 %all-reduce.1 = (f32[4,16,128]{2,1,0:T(8,128)S(1)}, bf16[4,2048]{1,0:T(4,128)(2,1)S(1)}) all-reduce(f32[4,16,128]{2,1,0:T(8,128)S(1)} %bitcast.99, f32[4,2048]{1,0:T(4,128)S(1)} %fusion.34), channel_id=1, replica_groups=mesh['gr'=2,'sp'=8,'tp'=2] {'sp'}, use_global_device_ids=true, to_apply=%region_9.10 | all-reduce | flops 16384 | bytes 114688 | tf_op jit(solution)/shard_map/psum | solution.py:94
  269.4 0.1 multiply_reduce_fusion
  269.5 0.1 multiply_bitcast_fusion
  269.6 0.6 fusion.30
  (25 shorter events, 0.3 us)
Async XLA Ops:
  7.2 137.0 %copy-start = (bf16[512,2048]{1,0:T(8,128)(2,1)S(1)}, bf16[512,2048]{1,0:T(8,128)(2,1)}, u32[]{:S(2)}) copy-start(bf16[512,2048]{1,0:T(8,128)(2,1)} %param.15) | copy-start | bytes 6291460
  7.2 21.9 %all-gather.2.cloned.1.call-start = ((), (), s32[]{:S(2)}) async-start(), calls=%async_computation.1 | async-start | bytes 9437184 | tf_op jit(solution)/shard_map/all_gather | solution.py:41
  7.9 223.5 %reduce-scatter.2.cloned.1.call-start = ((), (), s32[]{:S(2)}) async-start(), calls=%async_computation.2 | async-start | bytes 4718592 | tf_op jit(solution)/shard_map/reduce_scatter | solution.py:61
  47.6 3.9 %copy-start.8 = (bf16[768,4096]{1,0:T(8,128)(2,1)S(1)}, bf16[768,4096]{1,0:T(8,128)(2,1)}, u32[]{:S(2)}) copy-start(bf16[768,4096]{1,0:T(8,128)(2,1)} %all-gather.2.cloned.1.call-done) | copy-start | bytes 18874372
  68.3 2.8 %copy-start.1 = (f32[768,2048]{1,0:T(8,128)}, f32[768,2048]{1,0:T(8,128)S(1)}, u32[]{:S(2)}) copy-start(f32[768,2048]{1,0:T(8,128)S(1)} %add_divide_fusion) | copy-start | bytes 18874372
  68.3 2.8 copy-start.5
  119.4 3.2 %copy-start.2 = (f32[4,2048,2,128]{1,2,3,0:T(2,128)}, f32[4,2048,2,128]{1,2,3,0:T(2,128)S(1)}, u32[]{:S(2)}) copy-start(f32[4,2048,2,128]{1,2,3,0:T(2,128)S(1)} %fusion) | copy-start | bytes 25165828
  129.1 4.9 %copy-start.3 = (bf16[96,8,16,128]{3,2,1,0:T(8,128)(2,1)S(1)}, bf16[96,8,16,128]{3,2,1,0:T(8,128)(2,1)}, u32[]{:S(2)}) copy-start(bf16[96,8,16,128]{3,2,1,0:T(8,128)(2,1)} %copy.28) | copy-start | bytes 9437188
  134.0 6.3 %copy-start.6 = (bf16[4,512]{1,0:T(4,128)(2,1)S(1)}, bf16[4,512]{1,0:T(4,128)(2,1)}, u32[]{:S(2)}) copy-start(bf16[4,512]{1,0:T(4,128)(2,1)} %param.12) | copy-start | bytes 12292
  140.2 129.3 %copy-start.7 = (f32[128]{0:T(128)S(1)}, f32[128]{0:T(128)}, u32[]{:S(2)}) copy-start(f32[128]{0:T(128)} %param.19) | copy-start | bytes 1540
  232.5 37.8 %copy-start.4 = (bf16[4,16,16,128]{3,2,1,0:T(8,128)(2,1)}, bf16[4,16,16,128]{3,2,1,0:T(8,128)(2,1)S(1)}, u32[]{:S(2)}) copy-start(bf16[4,16,16,128]{3,2,1,0:T(8,128)(2,1)S(1)} %convert_element_type.48) | copy-start | bytes 786436
Sparse Core Ops, SparseCore 0:
  9.5 19.4 all-gather.1
  140.3 91.0 reduce-scatter.1
where the time goes:
time: 278 us; the launch traced here: 277 us
  blocking collectives  109 us (39%)
  waiting for transfers between devices  53.1 us (19%)
  matrix products  48.5 us (17%)
  local copies, waits for them, and re-layouts  28.2 us (10%)
  other arithmetic  24 us (9%)
  between operations  14.3 us (5%)
    reduce_scatter x1, waiting for transfers between devices, per_device(): lax.psum_scatter(state_terms, 'sp', scatter_dimension=2, tiled=True)  43.5 us
    psum x1, blocking collectives, per_device(): lax.psum((jnp.dot(first_token_input, query_weight, preferred_element_type...  41 us
    psum x1, blocking collectives, per_device(): read_sum = lax.psum(read_part, 'sp')  36.3 us
    all_gather x1, blocking collectives, carried_in(): pieces = lax.all_gather(value, axis)  31.3 us
    dot_general x1, matrix products, per_device(): jnp.dot(segment, value_weight, preferred_element_type=jnp.float32)  18.5 us
    dot_general x1, matrix products, per_device(): jnp.dot(segment, forget_weight, preferred_element_type=jnp.float32)  16.8 us
    another operation x3, other arithmetic  12 us
    unnamed x25, local copies, waits for them, and re-layouts  11 us
  transfers between devices with their start and end apart: 2, of which 2 were waited for; matrix products, arithmetic and copies ran while one was open for 7% of the time, Pallas kernels for 0%

commit v1 on v0

v1 whole, which is shorter than its diff:
```python
import functools

import jax
import jax.numpy as jnp
from jax import lax
from jax.experimental import pallas as pl
from jax.experimental.pallas import tpu as pltpu
from jax.sharding import PartitionSpec as P

F32 = jnp.float32
BF16 = jnp.bfloat16
GROUP_HEADS = 2
XROWS = 16


def kernel(
    dims,
    tokens,
    x_pad,
    qw,
    gw,
    wf,
    wv,
    slack,
    damp,
    scale,
    cache,
    first,
    seg,
    qw_s,
    gw_s,
    f_s,
    wk_s,
    v_s,
    nk_s,
    nv_s,
    tot,
    totr,
    later_s,
    qg,
    qgr,
    buf_a,
    rec_a,
    buf_b,
    rec_b,
    wt_s,
    rd,
    rdr,
    loc_sem,
    tok_ss,
    tok_rs,
    x_ss,
    x_rs,
    t_ss,
    t_rs,
    q_ss,
    q_rs,
    a_ss,
    a_rs,
    b_ss,
    b_rs,
    r_ss,
    r_rs,
):
    n, tp, seqs, length, groups, hd = dims
    hg = GROUP_HEADS
    width = hg * hd
    rows = seqs * length
    nz = n // 2
    own = hd // n
    g = pl.program_id(0)
    me = lax.axis_index("sp")
    tme = lax.axis_index("tp")
    y = lax.rem(me, 2)
    z = me // 2
    dp = tokens.shape[1]
    xw = x_pad.shape[1]

    def rcopy(src, dst, ss, rs, where):
        return pltpu.make_async_remote_copy(
            src_ref=src,
            dst_ref=dst,
            send_sem=ss,
            recv_sem=rs,
            device_id=where,
            device_id_type=pl.DeviceIdType.MESH,
        )

    gr = lax.axis_index("gr")

    def at_sp(p):
        return (gr, p, tme)

    def at_tp(t):
        return (gr, me, t)

    def up(d):
        return lax.rem(me + d, n)

    def seg_tok(t):
        return seg.at[pl.ds(0, rows), pl.ds(pl.multiple_of(t * dp, dp), dp)]

    def seg_x(p):
        return seg.at[pl.ds(rows, XROWS), pl.ds(pl.multiple_of(p * xw, xw), xw)]

    def tok_copy(d):
        return rcopy(tokens, seg_tok(tme), tok_ss.at[d - 1], tok_rs.at[d - 1], at_tp(lax.rem(tme + d, tp)))

    def x_copy(d):
        return rcopy(x_pad, seg_x(me), x_ss.at[d - 1], x_rs.at[d - 1], at_sp(up(d)))

    def local(k):
        src, dst = [(tokens, seg_tok(tme)), (x_pad, seg_x(me)), (qw, qw_s), (gw, gw_s)][k]
        return pltpu.make_async_copy(src, dst, loc_sem.at[k])

    def t_copy(k, d):
        return rcopy(tot.at[k], totr.at[k, d - 1], t_ss.at[k, d - 1], t_rs.at[k, d - 1], at_sp(up(d)))

    def q_copy(d):
        return rcopy(qg, qgr.at[d - 1], q_ss.at[d - 1], q_rs.at[d - 1], at_sp(up(d)))

    def a_copy(k):
        return rcopy(buf_a.at[k, 1 - y], rec_a.at[k], a_ss.at[k], a_rs.at[k], at_sp(me + 1 - 2 * y))

    def b_copy(k, d):
        there = lax.rem(z + d, nz)
        return rcopy(buf_b.at[k, there], rec_b.at[k, d - 1], b_ss.at[k, d - 1], b_rs.at[k, d - 1], at_sp(2 * there + y))

    def r_copy(k, d):
        return rcopy(rd.at[k], rdr.at[k, d - 1], r_ss.at[k, d - 1], r_rs.at[k, d - 1], at_sp(up(d)))

    @pl.when(g == 0)
    def _():
        local(0).start()
        local(1).start()
        barrier = pltpu.get_barrier_semaphore()
        for d in range(1, n):
            pl.semaphore_signal(barrier, inc=1, device_id=at_sp(up(d)), device_id_type=pl.DeviceIdType.MESH)
        for d in range(1, tp):
            pl.semaphore_signal(
                barrier, inc=1, device_id=at_tp(lax.rem(tme + d, tp)), device_id_type=pl.DeviceIdType.MESH
            )
        pl.semaphore_wait(barrier, n - 1 + tp - 1)
        for d in range(1, n):
            x_copy(d).start()
        for d in range(1, tp):
            tok_copy(d).start()
        local(2).start()
        local(3).start()
        local(0).wait()
        local(1).wait()
        for d in range(1, n):
            x_copy(d).wait_recv()

    for r in range(tp):
        if r > 0:

            @pl.when(g == 0)
            def _():
                tok_copy(tp - r).wait_recv()

        cut = pl.ds(pl.multiple_of(lax.rem(tme + r, tp) * dp, dp), dp)
        part = jnp.dot(seg[:, cut], wf[cut, :], preferred_element_type=F32)
        if r == 0:
            f_s[...] = part
        else:
            f_s[...] += part

    slot = lax.rem(g, 2)
    gap = slack[0]
    later_than = (
        lax.broadcasted_iota(jnp.int32, (length, length), 1) > lax.broadcasted_iota(jnp.int32, (length, length), 0)
    ).astype(BF16)
    for s in range(seqs):
        f = f_s[pl.ds(s * length, length), :].astype(BF16).astype(F32)
        keys = gap * jax.nn.sigmoid(-f)
        damping = damp[0, pl.ds(s * length, length), :]
        wide = jnp.concatenate([jnp.broadcast_to(damping[:, h : h + 1], (length, hd)) for h in range(hg)], axis=1)
        decay = jnp.log1p(-keys) + wide
        high = decay.astype(BF16)
        low = (decay - high.astype(F32)).astype(BF16)
        within = jnp.dot(later_than, high, preferred_element_type=F32) + jnp.dot(
            later_than, low, preferred_element_type=F32
        )
        wk_s[slot, pl.ds(s * length, length), :] = keys * jnp.exp(within)
        tot[g, pl.ds(s, 1), :] = within[0:1, :] + decay[0:1, :]
    for d in range(1, n):

        @pl.when(me + d >= n)
        def _():
            t_copy(g, d).start()

    nk_s[g] = gap * jax.nn.sigmoid(-f_s[pl.ds(rows, 8), :].astype(BF16).astype(F32))

    v = jnp.dot(seg[...], wv[...], preferred_element_type=F32).astype(BF16)
    v_s[slot] = v[:rows]
    nv_s[g] = v[rows:, :].astype(F32)

    @pl.when(g == 0)
    def _():
        local(2).wait()
        local(3).wait()
        xq = x_pad[...]
        qg[0:seqs, :] = jnp.dot(xq, qw_s[...], preferred_element_type=F32)[:seqs].astype(BF16)
        qg[seqs : 2 * seqs, :] = jnp.dot(xq, gw_s[...], preferred_element_type=F32)[:seqs].astype(BF16)
        for d in range(1, n):
            q_copy(d).start()

    def states(k):
        ks = lax.rem(k, 2)
        later_s[...] = jnp.zeros_like(later_s)
        for d in range(1, n):

            @pl.when(d > me)
            def _():
                t_copy(k, d).wait_recv()
                later_s[...] += totr[k, d - 1]

        faded = jnp.exp(later_s[...])
        for s in range(seqs):
            cut = pl.ds(s * length, length)
            w = (wk_s[ks, cut, :] * faded[s : s + 1, :]).astype(BF16)
            st = lax.dot_general(w, v_s[ks, cut, :], (((0,), (0,)), ((), ())), preferred_element_type=F32)
            for h in range(hg):
                block = st[h * hd : (h + 1) * hd, h * hd : (h + 1) * hd].astype(BF16)
                for p in range(n):
                    buf_a[k, p % 2, p // 2, s, h] = block[p * own : (p + 1) * own, :]
        a_copy(k).start()

    def pair(k):
        a_copy(k).wait_recv()
        buf_b[k] = (buf_a[k, y].astype(F32) + rec_a[k].astype(F32)).astype(BF16)
        for d in range(1, nz):
            b_copy(k, d).start()

    def query_gate(k):
        cut = pl.ds(pl.multiple_of(k * width, width), width)
        both = qg[:, cut].astype(F32)
        for d in range(1, n):
            both = both + qgr[d - 1, :, cut].astype(F32)
        return both.astype(BF16).astype(F32)

    def finish(k):
        total = buf_b[k, z].astype(F32)
        for d in range(1, nz):
            b_copy(k, d).wait_recv()
            total = total + rec_b[k, d - 1].astype(F32)
        kept = total.astype(BF16)
        q = query_gate(k)[:seqs]
        nk = nk_s[k, 0:seqs, :]
        fill = jnp.zeros((128 - 2 * seqs, width), F32)
        wt_s[...] = jnp.concatenate([q * (1.0 - nk), q * nk, fill], axis=0).T
        for h in range(hg):
            for s in range(seqs):
                cache[s, k * hg + h] = kept[s, h]
                mine = wt_s[pl.ds(pl.multiple_of(h * hd + me * own, own), own), :]
                old = jnp.sum(mine[:, s : s + 1] * kept[s, h].astype(F32), axis=0, keepdims=True)
                new = jnp.sum(
                    mine[:, seqs + s : seqs + s + 1] * nv_s[k, s : s + 1, h * hd : (h + 1) * hd], axis=0, keepdims=True
                )
                rd[k, s : s + 1, h * hd : (h + 1) * hd] = old + new
        for d in range(1, n):
            r_copy(k, d).start()

    def close(k):
        total = rd[k]
        for d in range(1, n):
            r_copy(k, d).wait_recv()
            total = total + rdr[k, d - 1]
        gate = query_gate(k)[seqs:]
        parts = []
        for h in range(hg):
            one = total[:, h * hd : (h + 1) * hd]
            parts.append(one * lax.rsqrt(jnp.mean(one * one, axis=-1, keepdims=True) + 1e-06) * scale[...])
        out = jnp.concatenate(parts, axis=1) * (gate * jax.nn.sigmoid(gate))
        first[:, pl.ds(pl.multiple_of(k * width, width), width)] = out.astype(BF16)

    def gathered():
        for d in range(1, n):
            q_copy(d).wait_recv()

    @pl.when(g >= 1)
    def _():
        states(g - 1)

    @pl.when(g >= 2)
    def _():
        pair(g - 2)

    if groups > 3:

        @pl.when(g == 3)
        def _():
            gathered()

        @pl.when(g >= 3)
        def _():
            finish(g - 3)

    @pl.when(g == groups - 1)
    def _():
        states(groups - 1)
        if groups <= 3:
            gathered()
        for k in range(max(groups - 2, 0), groups):
            pair(k)

        @pl.loop(max(groups - 3, 0), groups)
        def _(k):
            finish(k)

        @pl.loop(0, groups)
        def _(k):
            close(k)

        for d in range(1, n):
            x_copy(d).wait_send()
            q_copy(d).wait_send()
        for d in range(1, tp):
            tok_copy(d).wait_send()

        @pl.loop(0, groups)
        def _(k):
            a_copy(k).wait_send()
            for d in range(1, nz):
                b_copy(k, d).wait_send()
            for d in range(1, n):
                r_copy(k, d).wait_send()

                @pl.when(me + d >= n)
                def _():
                    t_copy(k, d).wait_send()


def per_device(
    tokens,
    first_token_input,
    forget_weight,
    value_weight,
    query_weight,
    output_gate_weight,
    forget_bound_slack,
    additional_damping_exponent,
    read_norm_scale,
):
    seqs, length, dp = tokens.shape
    hd = read_norm_scale.shape[0]
    heads = additional_damping_exponent.shape[2]
    n, tp = lax.axis_size("sp"), lax.axis_size("tp")
    hg = GROUP_HEADS
    groups = heads // hg
    width = hg * hd
    channels = heads * hd
    rows = seqs * length
    features = forget_weight.shape[0]
    xw = first_token_input.shape[1]
    own = hd // n
    nz = n // 2
    x_pad = jnp.pad(first_token_input, ((0, XROWS - seqs), (0, 0)))
    damp = additional_damping_exponent.reshape(rows, groups, hg).transpose(1, 0, 2)
    slack = forget_bound_slack.reshape(groups, 1, width)
    anywhere = pl.BlockSpec(memory_space=pl.ANY)
    whole = pl.BlockSpec(memory_space=pltpu.VMEM)
    dma = pltpu.SemaphoreType.DMA
    return pl.pallas_call(
        functools.partial(kernel, (n, tp, seqs, length, groups, hd)),
        grid=(groups,),
        out_shape=(
            jax.ShapeDtypeStruct((seqs, heads, own, hd), BF16),
            jax.ShapeDtypeStruct((seqs, channels), BF16),
        ),
        in_specs=[
            anywhere,
            whole,
            anywhere,
            anywhere,
            pl.BlockSpec((features, width), lambda g: (0, g)),
            pl.BlockSpec((features, width), lambda g: (0, g)),
            pl.BlockSpec((1, 1, width), lambda g: (g, 0, 0)),
            pl.BlockSpec((1, rows, hg), lambda g: (g, 0, 0)),
            whole,
        ],
        out_specs=(whole, whole),
        scratch_shapes=[
            pltpu.VMEM((rows + XROWS, features), BF16),
            pltpu.VMEM((xw, channels), BF16),
            pltpu.VMEM((xw, channels), BF16),
            pltpu.VMEM((rows + XROWS, width), F32),
            pltpu.VMEM((2, rows, width), F32),
            pltpu.VMEM((2, rows, width), BF16),
            pltpu.VMEM((groups, 8, width), F32),
            pltpu.VMEM((groups, XROWS, width), F32),
            pltpu.VMEM((groups, seqs, width), F32),
            pltpu.VMEM((groups, n - 1, seqs, width), F32),
            pltpu.VMEM((seqs, width), F32),
            pltpu.VMEM((2 * seqs, channels), BF16),
            pltpu.VMEM((n - 1, 2 * seqs, channels), BF16),
            pltpu.VMEM((groups, 2, nz, seqs, hg, own, hd), BF16),
            pltpu.VMEM((groups, nz, seqs, hg, own, hd), BF16),
            pltpu.VMEM((groups, nz, seqs, hg, own, hd), BF16),
            pltpu.VMEM((groups, nz - 1, seqs, hg, own, hd), BF16),
            pltpu.VMEM((width, 128), F32),
            pltpu.VMEM((groups, seqs, width), F32),
            pltpu.VMEM((groups, n - 1, seqs, width), F32),
            dma((4,)),
            dma((tp - 1,)),
            dma((tp - 1,)),
            dma((n - 1,)),
            dma((n - 1,)),
            dma((groups, n - 1)),
            dma((groups, n - 1)),
            dma((n - 1,)),
            dma((n - 1,)),
            dma((groups,)),
            dma((groups,)),
            dma((groups, nz - 1)),
            dma((groups, nz - 1)),
            dma((groups, n - 1)),
            dma((groups, n - 1)),
        ],
        compiler_params=pltpu.CompilerParams(
            collective_id=0,
            has_side_effects=True,
            dimension_semantics=("arbitrary",),
            vmem_limit_bytes=60 * 1024 * 1024,
        ),
    )(
        tokens.reshape(rows, dp),
        x_pad,
        query_weight,
        output_gate_weight,
        forget_weight,
        value_weight,
        slack,
        damp,
        read_norm_scale.reshape(1, hd),
    )


def solution(mesh):
    placed = (
        P("gr", "sp", "tp"),
        P("gr", "sp"),
        P(None, "tp"),
        P(None, "tp"),
        P("sp", "tp"),
        P("sp", "tp"),
        P("tp"),
        P("gr", "sp", "tp"),
        P(),
    )
    return jax.shard_map(
        per_device,
        mesh=mesh,
        in_specs=placed,
        out_specs=(P("gr", "tp", "sp", None), P("gr", "tp")),
        check_vma=False,
    )
```

time: 278 us -> 109 us (0.39)
  blocking collectives: 109 us -> 0 us
  Pallas kernels: 0 us -> 101 us
  waiting for transfers between devices: 53.1 us -> 0 us
  matrix products: 48.5 us -> 0 us
  other arithmetic: 24 us -> 0 us
  local copies, waits for them, and re-layouts: 28.2 us -> 7.51 us
  between operations: 14.3 us -> 0.64 us
    pallas_call x0 -> x1, Pallas kernels: none -> 101 us  [per_device(): pl.pallas_call(functools.partial(kernel, (n, tp, seqs, length, groups, hd...]
    psum x2 -> x0, blocking collectives: 77.3 us -> none  [the longest x1 41 us: per_device(): lax.psum((jnp.dot(first_token_input, query_weight, preferred_element_type...]
    dot_general x8 -> x0, matrix products: 48.5 us -> none  [the longest x1 18.5 us: per_device(): jnp.dot(segment, value_weight, preferred_element_type=jnp.float32)]
    reduce_scatter x1 -> x0, waiting for transfers between devices: 43.5 us -> none  [per_device(): lax.psum_scatter(state_terms, 'sp', scatter_dimension=2, tiled=True)]
    all_gather x1 -> x0, blocking collectives: 31.3 us -> none  [carried_in(): pieces = lax.all_gather(value, axis)]
    another operation x3 -> x0, other arithmetic: 12 us -> none
    all_gather x1 -> x0, waiting for transfers between devices: 8.95 us -> none  [per_device(): segment = lax.all_gather(flat_rows, 'tp', axis=1, tiled=True)]
    unnamed x25 -> x3, local copies, waits for them, and re-layouts: 11 us -> 3.88 us
  transfers between devices with their start and end apart: 2 -> 0, of which waited for: 2 -> 0; matrix products, arithmetic and copies ran while one was open for 7% -> 0% of each run, Pallas kernels for 0% -> 0%
where the time goes in v1:
time: 109 us
  Pallas kernels  101 us (93%)
  local copies, waits for them, and re-layouts  7.51 us (7%)
    pallas_call x1, Pallas kernels, per_device(): pl.pallas_call(functools.partial(kernel, (n, tp, seqs, length, groups, hd...  101 us
    unnamed x3, local copies, waits for them, and re-layouts  3.88 us
    reshape x2, local copies, waits for them, and re-layouts, per_device(): additional_damping_exponent.reshape(rows, groups, hg).transpose(1, 0, 2)  2.33 us

profile of v1, /device:TPU:0, one launch (start us, length us, event | category | flops | bytes accessed | tf_op | source)
XLA Modules:
  0.0 108.8 jit_solution(16352811905261908985)
XLA Ops:
  0.6 1.3 %pad.4.x_pad = bf16[16,512]{1,0:T(8,128)(2,1)} pad(bf16[4,512]{1,0:T(4,128)(2,1)} %param.10, bf16[]{:T(256)} %constant.2.clone.1), padding=0_12x0_0 | pad | bytes 20482 | tf_op jit(solution)/shard_map/jit(_pad)/pad | solution.py:359
  1.9 0.9 copy.11
  2.8 0.1 reshape.18
  2.9 2.2 %copy.12 = f32[768,8,2]{2,0,1:T(8,128)} copy(f32[768,8,2]{0,2,1:T(2,128)S(1)} %reshape.18) | data formatting | bytes 98304 | tf_op jit(solution)/shard_map/reshape | solution.py:360
  5.1 100.7 %shard_map.104 = (bf16[4,16,16,128]{3,2,1,0:T(8,128)(2,1)}, bf16[4,2048]{1,0:T(4,128)(2,1)}) custom-call(bf16[768,2048]{1,0:T(8,128)(2,1)} %bitcast.7, bf16[16,512]{1,0:T(8,128)(2,1)} %pad.4.x_pad, bf16[512,2048]{1,0:T(8,128)(2,1)} %qw.1, bf16[512,2048]{1,0:T(8,128)(2,1)} %gw.1, bf16[4096,2048]{1,0:T(8,128)(2,1)} %wf.1, bf16[4096,2048]{1,0:T(8,128)(2,1)} %wv.1, ...), custom_call_target="tpu_custom_call" | custom-call | tf_op jit(solution)/shard_map/pallas_call | solution.py:365
  105.8 1.7 %copy.15 = bf16[4,16,16,128]{3,2,1,0:T(8,128)(2,1)} copy(bf16[4,16,16,128]{3,2,1,0:T(8,128)(2,1)} %get-tuple-element.4) | data formatting | bytes 524288
  107.5 1.3 %copy.16 = bf16[4,2048]{1,0:T(4,128)(2,1)} copy(bf16[4,2048]{1,0:T(4,128)(2,1)} %get-tuple-element.5) | data formatting | bytes 32768

commit v2 on v1

--- a/solution.py
+++ b/solution.py
@@ -160,7 +160,8 @@
                 tok_copy(tp - r).wait_recv()
 
         cut = pl.ds(pl.multiple_of(lax.rem(tme + r, tp) * dp, dp), dp)
-        part = jnp.dot(seg[:, cut], wf[cut, :], preferred_element_type=F32)
+        both = jnp.concatenate([wf[cut, :], wv[cut, :]], axis=1)
+        part = jnp.dot(seg[:, cut], both, preferred_element_type=F32)
         if r == 0:
             f_s[...] = part
         else:
@@ -172,7 +173,7 @@
         lax.broadcasted_iota(jnp.int32, (length, length), 1) > lax.broadcasted_iota(jnp.int32, (length, length), 0)
     ).astype(BF16)
     for s in range(seqs):
-        f = f_s[pl.ds(s * length, length), :].astype(BF16).astype(F32)
+        f = f_s[pl.ds(s * length, length), :width].astype(BF16).astype(F32)
         keys = gap * jax.nn.sigmoid(-f)
         damping = damp[0, pl.ds(s * length, length), :]
         wide = jnp.concatenate([jnp.broadcast_to(damping[:, h : h + 1], (length, hd)) for h in range(hg)], axis=1)
@@ -190,9 +191,9 @@
         def _():
             t_copy(g, d).start()
 
-    nk_s[g] = gap * jax.nn.sigmoid(-f_s[pl.ds(rows, 8), :].astype(BF16).astype(F32))
-
-    v = jnp.dot(seg[...], wv[...], preferred_element_type=F32).astype(BF16)
+    nk_s[g] = gap * jax.nn.sigmoid(-f_s[pl.ds(rows, 8), :width].astype(BF16).astype(F32))
+
+    v = f_s[:, width:].astype(BF16)
     v_s[slot] = v[:rows]
     nv_s[g] = v[rows:, :].astype(F32)
 
@@ -302,12 +303,14 @@
         states(groups - 1)
         if groups <= 3:
             gathered()
-        for k in range(max(groups - 2, 0), groups):
-            pair(k)
-
-        @pl.loop(max(groups - 3, 0), groups)
-        def _(k):
-            finish(k)
+        if groups >= 2:
+            pair(groups - 2)
+        if groups >= 3:
+            finish(groups - 3)
+        pair(groups - 1)
+        if groups >= 2:
+            finish(groups - 2)
+        finish(groups - 1)
 
         @pl.loop(0, groups)
         def _(k):
@@ -385,7 +388,7 @@
             pltpu.VMEM((rows + XROWS, features), BF16),
             pltpu.VMEM((xw, channels), BF16),
             pltpu.VMEM((xw, channels), BF16),
-            pltpu.VMEM((rows + XROWS, width), F32),
+            pltpu.VMEM((rows + XROWS, 2 * width), F32),
             pltpu.VMEM((2, rows, width), F32),
             pltpu.VMEM((2, rows, width), BF16),
             pltpu.VMEM((groups, 8, width), F32),

time: 109 us -> 83.2 us (0.76)
  Pallas kernels: 101 us -> 74.8 us
    pallas_call x1, Pallas kernels: 101 us -> 74.8 us  [per_device(): pl.pallas_call(functools.partial(kernel, (n, tp, seqs, length, groups, hd...]
where the time goes in v2:
time: 83.2 us; the launch traced here: 82.9 us
  Pallas kernels  74.8 us (90%)
  local copies, waits for them, and re-layouts  7.51 us (9%)
    pallas_call x1, Pallas kernels, per_device(): pl.pallas_call(functools.partial(kernel, (n, tp, seqs, length, groups, hd...  74.8 us
    unnamed x3, local copies, waits for them, and re-layouts  3.88 us
    reshape x2, local copies, waits for them, and re-layouts, per_device(): additional_damping_exponent.reshape(rows, groups, hg).transpose(1, 0, 2)  2.33 us

profile of v2, /device:TPU:0, one launch (start us, length us, event | category | flops | bytes accessed | tf_op | source)
XLA Modules:
  0.0 82.9 jit_solution(4026257459274768305)
XLA Ops:
  0.6 1.3 %pad.4.x_pad = bf16[16,512]{1,0:T(8,128)(2,1)} pad(bf16[4,512]{1,0:T(4,128)(2,1)} %param.10, bf16[]{:T(256)} %constant.2.clone.1), padding=0_12x0_0 | pad | bytes 20482 | tf_op jit(solution)/shard_map/jit(_pad)/pad | solution.py:362
  1.9 0.9 %copy.11 = f32[4,192,16]{1,0,2:T(4,128)S(1)} copy(f32[4,192,16]{1,2,0:T(8,128)} %param.16) | data formatting | bytes 98304 | tf_op args[7]
  2.8 0.1 reshape.18
  2.9 2.2 %copy.12 = f32[768,8,2]{2,0,1:T(8,128)} copy(f32[768,8,2]{0,2,1:T(2,128)S(1)} %reshape.18) | data formatting | bytes 98304 | tf_op jit(solution)/shard_map/reshape | solution.py:363
  5.1 74.8 %shard_map.104 = (bf16[4,16,16,128]{3,2,1,0:T(8,128)(2,1)}, bf16[4,2048]{1,0:T(4,128)(2,1)}) custom-call(bf16[768,2048]{1,0:T(8,128)(2,1)} %bitcast.7, bf16[16,512]{1,0:T(8,128)(2,1)} %pad.4.x_pad, bf16[512,2048]{1,0:T(8,128)(2,1)} %qw.1, bf16[512,2048]{1,0:T(8,128)(2,1)} %gw.1, bf16[4096,2048]{1,0:T(8,128)(2,1)} %wf.1, bf16[4096,2048]{1,0:T(8,128)(2,1)} %wv.1, ...), custom_call_target="tpu_custom_call" | custom-call | tf_op jit(solution)/shard_map/pallas_call | solution.py:368
  79.9 1.7 %copy.15 = bf16[4,16,16,128]{3,2,1,0:T(8,128)(2,1)} copy(bf16[4,16,16,128]{3,2,1,0:T(8,128)(2,1)} %get-tuple-element.4) | data formatting | bytes 524288
  81.6 1.3 %copy.16 = bf16[4,2048]{1,0:T(4,128)(2,1)} copy(bf16[4,2048]{1,0:T(4,128)(2,1)} %get-tuple-element.5) | data formatting | bytes 32768
